TPU v7x, 128 devices: a whole 4x4x4 slice. The times are simulated.
128 devices in a mesh: ra: 16 (over z, x), cb: 8 (over y, core).
Axes of the slice: x: 4, y: 4, z: 4, core: 2. Of those that a mesh axis runs over, the one named last changes fastest.
Arguments:
- stream: bfloat16 [128, 2048], P(None, 'ra'), may hold values from -6 to 6
- gain_first: float32 [2048], P('ra'), may hold values from 0.5 to 1.5
- lift_first: bfloat16 [2048, 8192], P('ra', 'cb'), may hold values from -0.125 to 0.125
- drop_first: bfloat16 [8192, 2048], P('cb', 'ra'), may hold values from -0.0625 to 0.0625
- gain_second: float32 [2048], P('ra'), may hold values from 0.5 to 1.5
- lift_second: bfloat16 [2048, 8192], P('ra', 'cb'), may hold values from -0.125 to 0.125
- drop_second: bfloat16 [8192, 2048], P('cb', 'ra'), may hold values from -0.0625 to 0.0625
Outputs:
- stream_out: bfloat16 [128, 2048], P(None, 'ra')
All inputs are finite; a program needn't handle non-finite values.
Results may differ from a plain program's by a relative error of at most 0.0075.
Values may be sent and summed in bfloat16 or wider, within the bound.
A program may use at most 64 MiB of HBM per device.

v0:
```python
import jax
import jax.numpy as jnp
from jax import lax
from jax.sharding import Mesh
from jax.sharding import PartitionSpec as P

RA = ("ra_0", "ra_1")


residual_scale = 0.25
epsilon = 1e-06


def by_axis(shard, axes):
    for axis in axes:
        shard = lax.psum(shard, axis)
    return shard


def summed_rows(shard, axes, dim):
    if not axes:
        return shard
    nearer = lax.psum_scatter(shard, axes[0], scatter_dimension=dim, tiled=True)
    return summed_rows(nearer, axes[1:], dim)


def gathered_by_axis(shard, axes, dim):
    if not axes:
        return shard
    nearer = lax.all_gather(shard, axes[-1], axis=dim, tiled=True)
    return gathered_by_axis(nearer, axes[:-1], dim)


def taken_in(shard, axes, dim, update, carry):
    everything = jax.tree.map(lambda part: gathered_by_axis(part, axes, dim), shard)
    return update(carry, everything, jnp.int32(0))


def over_pieces(shard, axis):
    return lax.all_gather(shard, axis).sum(0)


def sublayer(stream, gain_vector, lift_weight, drop_weight):
    count_rows = stream.shape[0]
    tile_count = lax.axis_size(RA)
    feature_count = stream.shape[1] * tile_count
    widened = stream.astype(jnp.float32)
    local_squares = jnp.sum(widened * widened, axis=1, keepdims=True)
    gained = (widened * gain_vector.astype(jnp.float32)).astype(jnp.bfloat16)
    total_squares = by_axis(local_squares, RA)
    extras = ()
    products = jnp.dot(gained, lift_weight, preferred_element_type=jnp.float32)
    summed = jax.tree.map(lambda part: summed_rows(part, RA, 1), (products,) + extras)
    pre_act = summed[0]
    pre_act = pre_act * lax.rsqrt(total_squares / feature_count + epsilon)
    hidden = jnp.square(jnp.maximum(pre_act, 0.0)).astype(jnp.bfloat16)

    def add_rows(running, shard_piece, offset):
        weight_rows = lax.dynamic_slice_in_dim(drop_weight, offset, shard_piece.shape[1], 0)
        return running + jnp.dot(shard_piece, weight_rows, preferred_element_type=jnp.float32)

    initial = jnp.zeros((count_rows, drop_weight.shape[1]), jnp.float32)
    branch_part = taken_in(hidden, RA, 1, add_rows, initial)
    branch = over_pieces(branch_part, "cb")
    return (residual_scale * widened + branch).astype(jnp.bfloat16)


def per_device(stream, gain_first, lift_first, drop_first, gain_second, lift_second, drop_second):
    middle = sublayer(stream, gain_first, lift_first, drop_first)
    return sublayer(middle, gain_second, lift_second, drop_second)


def solution(mesh):
    finer = Mesh(mesh.devices.reshape(4, 4, mesh.shape["cb"]), ("ra_0", "ra_1", "cb"))
    in_specs = (P(None, RA), P(RA), P(RA, "cb"), P("cb", RA), P(RA), P(RA, "cb"), P("cb", RA))
    out_specs = P(None, RA)
    return jax.shard_map(
        per_device, mesh=finer, in_specs=in_specs, out_specs=out_specs, check_vma=False
    )
```

profile of v0, /device:TPU:1, one launch (start us, length us, event | category | flops | bytes accessed | tf_op | source)
XLA Modules:
  0.0 188.1 jit_solution(11467822812561255668)
XLA Ops:
  6.5 0.0 copy-start
  6.5 0.0 reduce-scatter.9.cloned.1.call-start
  6.5 0.9 copy-done
  7.5 1.8 fusion.10
  9.3 0.0 reduce-scatter.9.cloned.1.call-update
  9.3 0.0 reduce-scatter.13.cloned.1.call-start
  9.3 22.9 %reduce-scatter.9.cloned.1.call-done = f32[128,256]{1,0:T(8,128)} async-done(((f32[128,1024]{1,0:T(8,128)}), f32[128,256]{1,0:T(8,128)}) %reduce-scatter.9.cloned.1.call-update) | async-done | bytes 131088 | tf_op jit(solution)/shard_map/reduce_scatter | solution.py:23
  32.3 1.6 copy.12
  33.9 0.0 copy-start.1
  33.9 0.0 reduce-scatter.13.cloned.1.call-update
  33.9 0.0 copy-start.2
  33.9 0.0 reduce-scatter.11.cloned.1.call-start
  34.0 0.7 copy-done.1
  34.7 0.1 fusion.3
  34.8 7.1 %psum.28 = f32[128,1]{0,1:T(1,128)S(1)} all-reduce(f32[128,1]{0,1:T(1,128)S(1)} %bitcast.37), channel_id=1, replica_groups=mesh['ra_0'=4,'ra_1'=4,'cb'=8] {'ra_0'}, use_global_device_ids=true, to_apply=%region_3.0 | all-reduce | flops 128 | bytes 1024 | tf_op jit(solution)/shard_map/psum | solution.py:16
  41.9 8.8 %psum.29 = f32[128,1]{0,1:T(1,128)S(1)} all-reduce(f32[128,1]{0,1:T(1,128)S(1)} %psum.28), channel_id=1, replica_groups=mesh['ra_0'=4,'ra_1'=4,'cb'=8] {'ra_1'}, use_global_device_ids=true, to_apply=%region_4.0 | all-reduce | flops 128 | bytes 1024 | tf_op jit(solution)/shard_map/psum | solution.py:16
  50.7 4.4 %reduce-scatter.13.cloned.1.call-done = f32[64,128]{1,0:T(8,128)} async-done(((f32[256,128]{1,0:T(8,128)}), f32[64,128]{1,0:T(8,128)}) %reduce-scatter.13.cloned.1.call-update) | async-done | bytes 32784
  55.1 0.8 fusion.17
  55.9 9.0 %all_gather.24 = bf16[128,256]{0,1:T(8,128)(2,1)S(1)} all-gather(bf16[128,64]{0,1:T(8,128)(2,1)S(1)} %fusion.17), channel_id=1, replica_groups=mesh['ra_0'=4,'ra_1'=4,'cb'=8] {'ra_1'}, dimensions={1}, use_global_device_ids=true | all-gather | bytes 81920 | tf_op jit(solution)/shard_map/all_gather | solution.py:30
  64.8 10.1 %all_gather.25 = bf16[128,1024]{0,1:T(8,128)(2,1)S(1)} all-gather(bf16[128,256]{0,1:T(8,128)(2,1)S(1)} %all_gather.24), channel_id=1, replica_groups=mesh['ra_0'=4,'ra_1'=4,'cb'=8] {'ra_0'}, dimensions={1}, use_global_device_ids=true | all-gather | bytes 327680 | tf_op jit(solution)/shard_map/all_gather | solution.py:30
  75.0 0.0 copy-done.2
  75.0 0.3 fusion.21
  75.2 21.7 %all-gather = f32[1024,128]{1,0:T(8,128)S(1)} all-gather(f32[128,128]{1,0:T(8,128)S(1)} %fusion.21), channel_id=2, replica_groups=mesh['ra_0'=4,'ra_1'=4,'cb'=8] {'cb'}, dimensions={0}, use_global_device_ids=true | all-gather | bytes 589824 | tf_op jit(solution)/shard_map/all_gather | solution.py:40
  97.0 0.0 copy-start.4
  97.0 0.1 fusion.7
  97.1 0.0 copy-start.5
  97.1 0.8 copy-done.4
  97.9 0.0 copy-done.5
  97.9 1.0 fusion.8
  98.9 0.0 reduce-scatter.11.cloned.1.call-update
  98.9 0.0 reduce-scatter.15.cloned.1.call-start
  99.0 17.4 %reduce-scatter.11.cloned.1.call-done = f32[128,256]{1,0:T(8,128)} async-done(((f32[128,1024]{1,0:T(8,128)}), f32[128,256]{1,0:T(8,128)}) %reduce-scatter.11.cloned.1.call-update) | async-done | bytes 131088 | tf_op jit(solution)/shard_map/reduce_scatter | solution.py:23
  116.4 1.6 copy.14
  118.0 0.0 reduce-scatter.15.cloned.1.call-update
  118.0 0.0 copy-start.3
  118.0 7.3 %psum.30 = f32[128,1]{0,1:T(1,128)S(1)} all-reduce(f32[128,1]{0,1:T(1,128)S(1)} %bitcast.36), channel_id=1, replica_groups=mesh['ra_0'=4,'ra_1'=4,'cb'=8] {'ra_0'}, use_global_device_ids=true, to_apply=%region_9.0 | all-reduce | flops 128 | bytes 1024 | tf_op jit(solution)/shard_map/psum | solution.py:16
  125.3 8.4 %psum.31 = f32[128,1]{0,1:T(1,128)S(1)} all-reduce(f32[128,1]{0,1:T(1,128)S(1)} %psum.30), channel_id=1, replica_groups=mesh['ra_0'=4,'ra_1'=4,'cb'=8] {'ra_1'}, use_global_device_ids=true, to_apply=%region_10.0 | all-reduce | flops 128 | bytes 1024 | tf_op jit(solution)/shard_map/psum | solution.py:16
  133.7 5.3 %reduce-scatter.15.cloned.1.call-done = f32[64,128]{1,0:T(8,128)} async-done(((f32[256,128]{1,0:T(8,128)}), f32[64,128]{1,0:T(8,128)}) %reduce-scatter.15.cloned.1.call-update) | async-done | bytes 32784
  139.0 0.8 fusion.14
  139.8 9.0 %all_gather.28 = bf16[128,256]{0,1:T(8,128)(2,1)S(1)} all-gather(bf16[128,64]{0,1:T(8,128)(2,1)S(1)} %fusion.14), channel_id=1, replica_groups=mesh['ra_0'=4,'ra_1'=4,'cb'=8] {'ra_1'}, dimensions={1}, use_global_device_ids=true | all-gather | bytes 81920 | tf_op jit(solution)/shard_map/all_gather | solution.py:30
  148.8 10.1 %all_gather.29 = bf16[128,1024]{0,1:T(8,128)(2,1)S(1)} all-gather(bf16[128,256]{0,1:T(8,128)(2,1)S(1)} %all_gather.28), channel_id=1, replica_groups=mesh['ra_0'=4,'ra_1'=4,'cb'=8] {'ra_0'}, dimensions={1}, use_global_device_ids=true | all-gather | bytes 327680 | tf_op jit(solution)/shard_map/all_gather | solution.py:30
  158.9 0.0 copy-done.3
  158.9 0.3 fusion.22
  159.2 21.7 %all-gather.1 = f32[1024,128]{1,0:T(8,128)S(1)} all-gather(f32[128,128]{1,0:T(8,128)S(1)} %fusion.22), channel_id=3, replica_groups=mesh['ra_0'=4,'ra_1'=4,'cb'=8] {'cb'}, dimensions={0}, use_global_device_ids=true | all-gather | bytes 589824 | tf_op jit(solution)/shard_map/all_gather | solution.py:40
  181.0 0.6 fusion.5
  (4 shorter events, 0.1 us)
Async XLA Ops:
  6.5 1.0 copy-start
  6.5 25.7 %reduce-scatter.9.cloned.1.call-start = ((), (), s32[]{:S(2)}) async-start(), calls=%async_computation.4 | async-start | bytes 655360 | tf_op jit(solution)/shard_map/reduce_scatter | solution.py:23
  9.3 45.8 %reduce-scatter.13.cloned.1.call-start = ((), (), s32[]{:S(2)}) async-start(), calls=%async_computation.6 | async-start | bytes 163840
  33.9 0.8 copy-start.1
  33.9 41.0 %copy-start.2 = (bf16[1024,128]{1,0:T(8,128)(2,1)S(1)}, bf16[1024,128]{1,0:T(8,128)(2,1)}, u32[]{:S(2)}) copy-start(bf16[1024,128]{1,0:T(8,128)(2,1)} %param.10) | copy-start | bytes 786436
  33.9 82.4 %reduce-scatter.11.cloned.1.call-start = ((), (), s32[]{:S(2)}) async-start(), calls=%async_computation.5 | async-start | bytes 655360 | tf_op jit(solution)/shard_map/reduce_scatter | solution.py:23
  97.0 1.0 copy-start.4
  97.1 0.8 copy-start.5
  98.9 40.1 %reduce-scatter.15.cloned.1.call-start = ((), (), s32[]{:S(2)}) async-start(), calls=%async_computation.7 | async-start | bytes 163840
  118.0 40.9 %copy-start.3 = (bf16[1024,128]{1,0:T(8,128)(2,1)S(1)}, bf16[1024,128]{1,0:T(8,128)(2,1)}, u32[]{:S(2)}) copy-start(bf16[1024,128]{1,0:T(8,128)(2,1)} %param.13) | copy-start | bytes 786436
Sparse Core Ops, SparseCore 0:
  9.7 22.5 reduce-scatter.8
  34.6 20.4 reduce-scatter.12
  99.1 17.2 reduce-scatter.10
  118.6 20.4 reduce-scatter.14
where the time goes:
time: 189 us; the launch traced here: 188 us
  blocking collectives  113 us (60%)
  waiting for transfers between devices  50 us (26%)
  between operations  13.2 us (7%)
  local copies, waits for them, and re-layouts  5.71 us (3%)
  matrix products  3.3 us (2%)
  other arithmetic  2.44 us (1%)
    all_gather x2, blocking collectives, over_pieces(): return lax.all_gather(shard, axis).sum(0)  43.4 us
    reduce_scatter x2, waiting for transfers between devices, summed_rows(): nearer = lax.psum_scatter(shard, axes[0], scatter_dimension=dim, tiled=True)  40.3 us
    all_gather x4, blocking collectives, gathered_by_axis(): nearer = lax.all_gather(shard, axes[-1], axis=dim, tiled=True)  38.2 us
    psum x4, blocking collectives, by_axis(): shard = lax.psum(shard, axis)  31.7 us
    unnamed x6, waiting for transfers between devices  9.73 us
    unnamed x14, local copies, waits for them, and re-layouts  5.71 us
  transfers between devices with their start and end apart: 4, of which 4 were waited for; matrix products, arithmetic and copies ran while one was open for 0% of the time, Pallas kernels for 0%

commit v1 on v0

v1 whole, which is shorter than its diff:
```python
import functools

import jax
import jax.numpy as jnp
from jax import lax
from jax.experimental import pallas as pl
from jax.experimental.pallas import tpu as pltpu
from jax.sharding import PartitionSpec as P

MESH = pl.DeviceIdType.MESH
F32 = jnp.float32
BF16 = jnp.bfloat16

residual_scale = 0.25
epsilon = 1e-06

SIDE = 4
RA = SIDE * SIDE
FEATURES = 2048

OFFSETS = sorted(
    [(dz, dx) for dz in range(SIDE) for dx in range(SIDE) if (dz, dx) != (0, 0)],
    key=lambda o: -(min(o[0], SIDE - o[0]) + min(o[1], SIDE - o[1])),
)


def kernel(
    stream_hbm, gain1_hbm, lift1_hbm, drop1_hbm, gain2_hbm, lift2_hbm, drop2_hbm, out_ref,
    stream, gain, lift, drop, part, part_in, hid, branch, branch_in, pair, pair_in, sq, sq_in,
    load_sem, part_ssem, part_rsem, hid_ssem, hid_rsem, br_ssem, br_rsem, pair_ssem, pair_rsem, sq_ssem, sq_rsem,
):
    ra = lax.axis_index("ra")
    cb = lax.axis_index("cb")
    z, x = ra // SIDE, ra % SIDE
    y, core = cb // 2, cb % 2
    half = part.shape[2]

    loads = [
        pltpu.make_async_copy(src, dst, load_sem.at[i])
        for i, (src, dst) in enumerate([
            (stream_hbm, stream), (gain1_hbm, gain.at[0]), (lift1_hbm, lift.at[0]), (drop1_hbm, drop.at[0]),
            (gain2_hbm, gain.at[1]), (lift2_hbm, lift.at[1]), (drop2_hbm, drop.at[1]),
        ])
    ]
    for load in loads:
        load.start()

    peers = [lax.rem(z + dz, SIDE) * SIDE + lax.rem(x + dx, SIDE) for dz, dx in OFFSETS]
    columns = [lax.rem(y + dy, SIDE) * 2 + core for dy in (2, 1, 3)]
    partner = cb + 1 - 2 * core

    barrier = pltpu.get_barrier_semaphore()
    for peer in peers:
        pl.semaphore_signal(barrier, inc=1, device_id=(peer, cb), device_id_type=MESH)
    for column in columns:
        pl.semaphore_signal(barrier, inc=1, device_id=(ra, column), device_id_type=MESH)
    pl.semaphore_signal(barrier, inc=1, device_id=(ra, partner), device_id_type=MESH)

    pending = []

    def send(src, dst, ssem, rsem, device):
        copy = pltpu.make_async_remote_copy(
            src_ref=src, dst_ref=dst, send_sem=ssem, recv_sem=rsem, device_id=device, device_id_type=MESH
        )
        copy.start()
        pending.append(copy)

    def arrive(dst, ssem, rsem):
        pltpu.make_async_remote_copy(
            src_ref=dst, dst_ref=dst, send_sem=ssem, recv_sem=rsem, device_id=(ra, cb), device_id_type=MESH
        ).wait_recv()

    loads[0].wait()
    loads[1].wait()
    current = stream[...].astype(F32)
    for layer in range(2):
        if layer == 1:
            loads[4].wait()
        gained = (current * gain[layer]).astype(BF16)
        squares = current * current
        sq[layer] = jnp.sum(squares.T, axis=0, keepdims=True)
        loads[2 + 3 * layer].wait()
        products = jnp.dot(gained, lift[layer], preferred_element_type=F32)
        for i in range(RA):
            rows, cols = i // 8, i % 8
            part[layer, i] = products[rows * half:(rows + 1) * half, cols * 128:(cols + 1) * 128].astype(BF16)
        if layer == 0:
            pl.semaphore_wait(barrier, RA - 1 + SIDE)
        for k, peer in enumerate(peers):
            send(part.at[layer, peer], part_in.at[layer, ra], part_ssem.at[layer, k], part_rsem.at[layer, ra], (peer, cb))
        for k, peer in enumerate(peers):
            send(sq.at[layer], sq_in.at[layer, ra], sq_ssem.at[layer, k], sq_rsem.at[layer, ra], (peer, cb))

        total = part[layer, ra].astype(F32)
        for k in reversed(range(RA - 1)):
            peer = peers[k]
            arrive(part_in.at[layer, peer], part_ssem.at[layer, k], part_rsem.at[layer, peer])
            total += part_in[layer, peer].astype(F32)
        positive = jnp.maximum(total, 0.0)
        hid[layer, ra] = (positive * positive).astype(BF16)
        for k, peer in enumerate(peers):
            send(hid.at[layer, ra], hid.at[layer, ra], hid_ssem.at[layer, k], hid_rsem.at[layer, ra], (peer, cb))

        sq_in[layer, ra] = sq[layer]
        for k in range(RA - 1):
            arrive(sq_in.at[layer, peers[k]], sq_ssem.at[layer, k], sq_rsem.at[layer, peers[k]])
        sums = sq_in[layer, 0]
        for i in range(1, RA):
            sums += sq_in[layer, i]
        scale = jnp.broadcast_to(1.0 / (sums / FEATURES + epsilon), (128, 128)).T

        loads[3 + 3 * layer].wait()
        for k in reversed(range(RA - 1)):
            peer = peers[k]
            arrive(hid.at[layer, peer], hid_ssem.at[layer, k], hid_rsem.at[layer, peer])
        for rows in range(2):
            hidden = jnp.concatenate([hid[layer, rows * 8 + i] for i in range(8)], axis=1)
            mine = jnp.dot(hidden, drop[layer], preferred_element_type=F32)
            branch[layer, rows * half:(rows + 1) * half] = mine.astype(BF16)
        for k, column in enumerate(columns):
            send(branch.at[layer], branch_in.at[layer, y], br_ssem.at[layer, k], br_rsem.at[layer, y], (ra, column))
        branch_in[layer, y] = branch[layer]
        for k, column in reversed(list(enumerate(columns))):
            arrive(branch_in.at[layer, column // 2], br_ssem.at[layer, k], br_rsem.at[layer, column // 2])
        summed = branch_in[layer, 0].astype(F32)
        for i in range(1, SIDE):
            summed += branch_in[layer, i].astype(F32)
        pair[layer] = summed
        send(pair.at[layer], pair_in.at[layer], pair_ssem.at[layer], pair_rsem.at[layer], (ra, partner))
        arrive(pair_in.at[layer], pair_ssem.at[layer], pair_rsem.at[layer])
        after = (residual_scale * current + scale * (summed + pair_in[layer])).astype(BF16)
        current = after.astype(F32)

    out_ref[...] = after
    for copy in pending:
        copy.wait_send()


def per_device(stream, gain_first, lift_first, drop_first, gain_second, lift_second, drop_second):
    tokens, width = stream.shape
    hidden = lift_first.shape[1]
    any_spec = pl.BlockSpec(memory_space=pl.ANY)
    dma = pltpu.SemaphoreType.DMA
    return pl.pallas_call(
        kernel,
        out_shape=jax.ShapeDtypeStruct((tokens, width), BF16),
        in_specs=[any_spec] * 7,
        out_specs=pl.BlockSpec(memory_space=pltpu.VMEM),
        scratch_shapes=[
            pltpu.VMEM((tokens, width), BF16),
            pltpu.VMEM((2, 1, width), F32),
            pltpu.VMEM((2, width, hidden), BF16),
            pltpu.VMEM((2, hidden, width), BF16),
            pltpu.VMEM((2, RA, tokens // 2, 128), BF16),
            pltpu.VMEM((2, RA, tokens // 2, 128), BF16),
            pltpu.VMEM((2, RA, tokens // 2, 128), BF16),
            pltpu.VMEM((2, tokens, width), BF16),
            pltpu.VMEM((2, SIDE, tokens, width), BF16),
            pltpu.VMEM((2, tokens, width), F32),
            pltpu.VMEM((2, tokens, width), F32),
            pltpu.VMEM((2, 1, tokens), F32),
            pltpu.VMEM((2, RA, 1, tokens), F32),
            dma((7,)),
            dma((2, RA)), dma((2, RA)),
            dma((2, RA)), dma((2, RA)),
            dma((2, SIDE)), dma((2, SIDE)),
            dma((2,)), dma((2,)),
            dma((2, RA)), dma((2, RA)),
        ],
        compiler_params=pltpu.CompilerParams(collective_id=0, has_side_effects=True),
        name="ffn_pair",
    )(
        stream, gain_first.reshape(1, width), lift_first, drop_first,
        gain_second.reshape(1, width), lift_second, drop_second,
    )


def solution(mesh):
    in_specs = (P(None, "ra"), P("ra"), P("ra", "cb"), P("cb", "ra"), P("ra"), P("ra", "cb"), P("cb", "ra"))
    return jax.shard_map(
        per_device, mesh=mesh, in_specs=in_specs, out_specs=P(None, "ra"), check_vma=False
    )
```

time: 189 us -> 47.4 us (0.25)
  blocking collectives: 113 us -> 0 us
  waiting for transfers between devices: 50 us -> 0 us
  Pallas kernels: 0 us -> 45.8 us
  between operations: 13.2 us -> 0.01 us
  local copies, waits for them, and re-layouts: 5.71 us -> 1.38 us
  matrix products: 3.3 us -> 0 us
  other arithmetic: 2.44 us -> 0 us
    all_gather x6 -> x0, blocking collectives: 81.6 us -> none  [the longest x2 43.4 us: over_pieces(): return lax.all_gather(shard, axis).sum(0)]
    pallas_call x0 -> x1, Pallas kernels: none -> 45.8 us  [per_device(): pl.pallas_call(kernel, out_shape=jax.ShapeDtypeStruct((tokens, width), BF...]
    reduce_scatter x2 -> x0, waiting for transfers between devices: 40.3 us -> none  [summed_rows(): nearer = lax.psum_scatter(shard, axes[0], scatter_dimension=dim, tiled=True)]
    psum x4 -> x0, blocking collectives: 31.7 us -> none  [by_axis(): shard = lax.psum(shard, axis)]
    unnamed x6 -> x0, waiting for transfers between devices: 9.73 us -> none
    unnamed x14 -> x1, local copies, waits for them, and re-layouts: 5.71 us -> 1.38 us
    dot_general x4 -> x0, matrix products: 3.3 us -> none  [the longest x2 2.77 us: sublayer(): products = jnp.dot(gained, lift_weight, preferred_element_type=jnp.float32)]
    convert_element_type x3 -> x0, other arithmetic: 2.16 us -> none  [the longest x2 1.53 us: sublayer(): hidden = jnp.square(jnp.maximum(pre_act, 0.0)).astype(jnp.bfloat16)]
  transfers between devices with their start and end apart: 4 -> 0, of which waited for: 4 -> 0; matrix products, arithmetic and copies ran while one was open for 0% -> 0% of each run, Pallas kernels for 0% -> 0%
where the time goes in v1:
time: 47.4 us; the launch traced here: 47.2 us
  Pallas kernels  45.8 us (97%)
  local copies, waits for them, and re-layouts  1.38 us (3%)
    pallas_call x1, Pallas kernels, per_device(): pl.pallas_call(kernel, out_shape=jax.ShapeDtypeStruct((tokens, width), BF...  45.8 us
    unnamed x1, local copies, waits for them, and re-layouts  1.38 us

profile of v1, /device:TPU:1, one launch (start us, length us, event | category | flops | bytes accessed | tf_op | source)
XLA Modules:
  0.0 47.2 jit_solution(3776287518630745697)
XLA Ops:
  0.0 45.8 %ffn_pair.1 = bf16[128,128]{1,0:T(8,128)(2,1)} custom-call(bf16[128,128]{1,0:T(8,128)(2,1)} %stream_hbm.1, f32[1,128]{1,0:T(1,128)} %bitcast.2, bf16[128,1024]{1,0:T(8,128)(2,1)} %lift1_hbm.1, bf16[1024,128]{1,0:T(8,128)(2,1)} %drop1_hbm.1, f32[1,128]{1,0:T(1,128)} %bitcast.3, bf16[128,1024]{1,0:T(8,128)(2,1)} %lift2_hbm.1, bf16[1024,128]{1,0:T(8,128)(2,1)} %drop2_hbm.1), custom_call_target="tpu_custom_call" | custom-call | tf_op jit(solution)/shard_map/ffn_pair/pallas_call | solution.py:144
  45.8 1.4 %copy.9 = bf16[128,128]{1,0:T(8,128)(2,1)} copy(bf16[128,128]{1,0:T(8,128)(2,1)} %ffn_pair.1) | data formatting | bytes 65536

commit v2 on v1

v2 whole, which is shorter than its diff:
```python
import jax
import jax.numpy as jnp
from jax import lax
from jax.experimental import pallas as pl
from jax.experimental.pallas import tpu as pltpu
from jax.sharding import PartitionSpec as P

MESH = pl.DeviceIdType.MESH
F32 = jnp.float32
BF16 = jnp.bfloat16

residual_scale = 0.25
epsilon = 1e-06

SIDE = 4
RA = SIDE * SIDE
CB = 2 * SIDE
FEATURES = 2048
LANES = 128
BLOCKS = 2
SPLIT = 2
GROUPS = RA // SPLIT

OFFSETS = sorted(
    [(dz, dx) for dz in range(SIDE) for dx in range(SIDE) if (dz, dx) != (0, 0)],
    key=lambda o: -(min(o[0], SIDE - o[0]) + min(o[1], SIDE - o[1])),
)
COLUMN_OFFSETS = [(2, 0), (2, 1), (1, 0), (1, 1), (3, 0), (3, 1), (0, 1)]


def kernel(
    stream_hbm, gain1_hbm, lift1_hbm, drop1_hbm, gain2_hbm, lift2_hbm, drop2_hbm, out_ref,
    stream, gain, lift, drop, part, part_in, hid, branch, sq, sq_in,
    load_sem, part_ssem, part_rsem, hid_ssem, hid_rsem, br_ssem, br_rsem, sq_ssem, sq_rsem,
):
    ra = lax.axis_index("ra")
    cb = lax.axis_index("cb")
    z, x = ra // SIDE, ra % SIDE
    y, core = cb // 2, cb % 2
    tokens = stream.shape[0]
    size = tokens // BLOCKS
    rows = size // SPLIT

    peers = [lax.rem(z + dz, SIDE) * SIDE + lax.rem(x + dx, SIDE) for dz, dx in OFFSETS]
    columns = [lax.rem(y + dy, SIDE) * 2 + lax.rem(core + dc, 2) for dy, dc in COLUMN_OFFSETS]

    barrier = pltpu.get_barrier_semaphore()
    for peer in peers:
        pl.semaphore_signal(barrier, inc=1, device_id=(peer, cb), device_id_type=MESH)
    for column in columns:
        pl.semaphore_signal(barrier, inc=1, device_id=(ra, column), device_id_type=MESH)

    loads = [
        pltpu.make_async_copy(src, dst, load_sem.at[i])
        for i, (src, dst) in enumerate([
            (stream_hbm, stream), (gain1_hbm, gain.at[0]), (lift1_hbm, lift.at[0]), (drop1_hbm, drop.at[0]),
            (gain2_hbm, gain.at[1]), (lift2_hbm, lift.at[1]), (drop2_hbm, drop.at[1]),
        ])
    ]
    for load in loads:
        load.start()

    def send(src, dst, ssem, rsem, device):
        pltpu.make_async_remote_copy(
            src_ref=src, dst_ref=dst, send_sem=ssem, recv_sem=rsem, device_id=device, device_id_type=MESH
        ).start()

    def arrived(ref, rsem):
        pltpu.make_async_copy(ref, ref, rsem).wait()

    def multiply_in(layer, b, current):
        gained = (current * gain[layer]).astype(BF16)
        products = jnp.dot(gained, lift[layer], preferred_element_type=F32).astype(BF16)
        for i in range(RA):
            r, c = i // GROUPS, i % GROUPS
            part[layer, b, i] = products[r * rows:(r + 1) * rows, c * LANES:(c + 1) * LANES]

    def scatter(layer, b):
        for k, peer in enumerate(peers):
            send(part.at[layer, b, peer], part_in.at[layer, b, k], part_ssem.at[layer, b], part_rsem.at[layer, b], (peer, cb))

    def send_squares(layer, current):
        sq[layer] = jnp.sum((current * current).T, axis=0, keepdims=True)
        for k, peer in enumerate(peers):
            send(sq.at[layer], sq_in.at[layer, k], sq_ssem.at[layer], sq_rsem.at[layer], (peer, cb))

    def activate(layer, b):
        arrived(part_in.at[layer, b], part_rsem.at[layer, b])
        total = part[layer, b, ra].astype(F32)
        for k in range(RA - 1):
            total += part_in[layer, b, k].astype(F32)
        positive = jnp.maximum(total, 0.0)
        hid[layer, b, ra] = (positive * positive).astype(BF16)
        for peer in peers:
            send(hid.at[layer, b, ra], hid.at[layer, b, ra], hid_ssem.at[layer, b], hid_rsem.at[layer, b], (peer, cb))

    def token_scale(layer):
        arrived(sq_in.at[layer], sq_rsem.at[layer])
        sums = sq[layer]
        for k in range(RA - 1):
            sums += sq_in[layer, k]
        return jnp.broadcast_to(1.0 / (sums / FEATURES + epsilon), (tokens, tokens)).T

    def multiply_out(layer, b):
        arrived(hid.at[layer, b, pl.ds(0, RA - 1)], hid_rsem.at[layer, b])
        hidden = jnp.concatenate([
            jnp.concatenate([hid[layer, b, r * GROUPS + c] for c in range(GROUPS)], axis=1) for r in range(SPLIT)
        ], axis=0)
        branch[layer, b, cb] = jnp.dot(hidden, drop[layer], preferred_element_type=F32).astype(BF16)
        for column in columns:
            send(branch.at[layer, b, cb], branch.at[layer, b, cb], br_ssem.at[layer, b], br_rsem.at[layer, b], (ra, column))

    def finish(layer, b, current, scale):
        arrived(branch.at[layer, b, pl.ds(0, CB - 1)], br_rsem.at[layer, b])
        total = branch[layer, b, 0].astype(F32)
        for i in range(1, CB):
            total += branch[layer, b, i].astype(F32)
        return (residual_scale * current + scale * total).astype(BF16)

    loads[0].wait()
    loads[1].wait()
    span = [slice(b * size, (b + 1) * size) for b in range(BLOCKS)]
    current = [stream[s].astype(F32) for s in span]
    loads[2].wait()
    for b in range(BLOCKS):
        multiply_in(0, b, current[b])
    pl.semaphore_wait(barrier, RA - 1 + CB - 1)
    for b in range(BLOCKS):
        scatter(0, b)
    send_squares(0, jnp.concatenate(current, axis=0))
    for layer in range(2):
        for b in range(BLOCKS):
            activate(layer, b)
        scale = token_scale(layer)
        loads[3 + 3 * layer].wait()
        for b in range(BLOCKS):
            multiply_out(layer, b)
        if layer == 0:
            loads[4].wait()
            loads[5].wait()
        after = []
        for b in range(BLOCKS):
            block = finish(layer, b, current[b], scale[span[b]])
            if layer == 0:
                after.append(block.astype(F32))
                multiply_in(1, b, after[b])
                scatter(1, b)
            else:
                out_ref[span[b]] = block
        if layer == 0:
            send_squares(1, jnp.concatenate(after, axis=0))
            current = after

    for layer in range(2):
        for b in range(BLOCKS):
            arrived(part_in.at[layer, b], part_ssem.at[layer, b])
            arrived(hid.at[layer, b, pl.ds(0, RA - 1)], hid_ssem.at[layer, b])
            arrived(branch.at[layer, b, pl.ds(0, CB - 1)], br_ssem.at[layer, b])
        arrived(sq_in.at[layer], sq_ssem.at[layer])


def per_device(stream, gain_first, lift_first, drop_first, gain_second, lift_second, drop_second):
    tokens, width = stream.shape
    hidden = lift_first.shape[1]
    size = tokens // BLOCKS
    rows = size // SPLIT
    any_spec = pl.BlockSpec(memory_space=pl.ANY)
    dma = pltpu.SemaphoreType.DMA
    return pl.pallas_call(
        kernel,
        out_shape=pltpu.VMEM((tokens, width), BF16),
        in_specs=[any_spec] * 7,
        out_specs=pl.BlockSpec(memory_space=pltpu.VMEM),
        scratch_shapes=[
            pltpu.VMEM((tokens, width), BF16),
            pltpu.VMEM((2, 1, width), F32),
            pltpu.VMEM((2, width, hidden), BF16),
            pltpu.VMEM((2, hidden, width), BF16),
            pltpu.VMEM((2, BLOCKS, RA, rows, LANES), BF16),
            pltpu.VMEM((2, BLOCKS, RA - 1, rows, LANES), BF16),
            pltpu.VMEM((2, BLOCKS, RA, rows, LANES), BF16),
            pltpu.VMEM((2, BLOCKS, CB, size, width), BF16),
            pltpu.VMEM((2, 1, tokens), F32),
            pltpu.VMEM((2, RA - 1, 1, tokens), F32),
            dma((7,)),
            dma((2, BLOCKS)), dma((2, BLOCKS)),
            dma((2, BLOCKS)), dma((2, BLOCKS)),
            dma((2, BLOCKS)), dma((2, BLOCKS)),
            dma((2,)), dma((2,)),
        ],
        compiler_params=pltpu.CompilerParams(collective_id=0, has_side_effects=True),
        name="ffn_pair",
    )(
        stream, gain_first.reshape(1, width), lift_first, drop_first,
        gain_second.reshape(1, width), lift_second, drop_second,
    )


def solution(mesh):
    in_specs = (P(None, "ra"), P("ra"), P("ra", "cb"), P("cb", "ra"), P("ra"), P("ra", "cb"), P("cb", "ra"))
    return jax.shard_map(
        per_device, mesh=mesh, in_specs=in_specs, out_specs=P(None, "ra"), check_vma=False
    )
```

time: 47.4 us -> 38.6 us (0.81)
  Pallas kernels: 45.8 us -> 37.9 us
  local copies, waits for them, and re-layouts: 1.38 us -> 0.62 us
    pallas_call x1, Pallas kernels: 45.8 us -> 37.9 us  [per_device(): pl.pallas_call(kernel, out_shape=pltpu.VMEM((tokens, width), BF16), in_sp...]
    unnamed x1, local copies, waits for them, and re-layouts: 1.38 us -> 0.62 us
where the time goes in v2:
time: 38.6 us; the launch traced here: 38.5 us
  Pallas kernels  37.9 us (98%)
  local copies, waits for them, and re-layouts  0.62 us (2%)
    pallas_call x1, Pallas kernels, per_device(): pl.pallas_call(kernel, out_shape=pltpu.VMEM((tokens, width), BF16), in_sp...  37.9 us

profile of v2, /device:TPU:1, one launch (start us, length us, event | category | flops | bytes accessed | tf_op | source)
XLA Modules:
  0.0 38.5 jit_solution(3483294034579631721)
XLA Ops:
  0.0 37.9 %ffn_pair.1 = bf16[128,128]{1,0:T(8,128)(2,1)S(1)} custom-call(bf16[128,128]{1,0:T(8,128)(2,1)} %stream_hbm.1, f32[1,128]{1,0:T(1,128)} %bitcast.2, bf16[128,1024]{1,0:T(8,128)(2,1)} %lift1_hbm.1, bf16[1024,128]{1,0:T(8,128)(2,1)} %drop1_hbm.1, f32[1,128]{1,0:T(1,128)} %bitcast.3, bf16[128,1024]{1,0:T(8,128)(2,1)} %lift2_hbm.1, bf16[1024,128]{1,0:T(8,128)(2,1)} %drop2_hbm.1), custom_call_target="tpu_custom_call" | custom-call | tf_op jit(solution)/shard_map/ffn_pair/pallas_call | solution.py:169
  37.9 0.6 %copy.9 = bf16[128,128]{1,0:T(8,128)(2,1)} copy(bf16[128,128]{1,0:T(8,128)(2,1)S(1)} %ffn_pair.1) | data formatting | bytes 65536

commit v3 on v2

--- a/solution.py
+++ b/solution.py
@@ -17,7 +17,7 @@
 CB = 2 * SIDE
 FEATURES = 2048
 LANES = 128
-BLOCKS = 2
+BLOCKS = 4
 SPLIT = 2
 GROUPS = RA // SPLIT
 

time: 38.6 us -> 37.8 us (0.979)
  Pallas kernels: 37.9 us -> 37.1 us
    pallas_call x1, Pallas kernels: 37.9 us -> 37.1 us  [per_device(): pl.pallas_call(kernel, out_shape=pltpu.VMEM((tokens, width), BF16), in_sp...]
where the time goes in v3:
time: 37.8 us; the launch traced here: 37.7 us
  Pallas kernels  37.1 us (98%)
  local copies, waits for them, and re-layouts  0.62 us (2%)
    pallas_call x1, Pallas kernels, per_device(): pl.pallas_call(kernel, out_shape=pltpu.VMEM((tokens, width), BF16), in_sp...  37.1 us

profile of v3, /device:TPU:1, one launch (start us, length us, event | category | flops | bytes accessed | tf_op | source)
XLA Modules:
  0.0 37.7 jit_solution(1571360372277537538)
XLA Ops:
  0.0 37.1 %ffn_pair.1 = bf16[128,128]{1,0:T(8,128)(2,1)S(1)} custom-call(bf16[128,128]{1,0:T(8,128)(2,1)} %stream_hbm.1, f32[1,128]{1,0:T(1,128)} %bitcast.2, bf16[128,1024]{1,0:T(8,128)(2,1)} %lift1_hbm.1, bf16[1024,128]{1,0:T(8,128)(2,1)} %drop1_hbm.1, f32[1,128]{1,0:T(1,128)} %bitcast.3, bf16[128,1024]{1,0:T(8,128)(2,1)} %lift2_hbm.1, bf16[1024,128]{1,0:T(8,128)(2,1)} %drop2_hbm.1), custom_call_target="tpu_custom_call" | custom-call | tf_op jit(solution)/shard_map/ffn_pair/pallas_call | solution.py:169
  37.1 0.6 %copy.9 = bf16[128,128]{1,0:T(8,128)(2,1)} copy(bf16[128,128]{1,0:T(8,128)(2,1)S(1)} %ffn_pair.1) | data formatting | bytes 65536
